TPU v7x, 256 devices: a whole 4x4x8 slice. The times are simulated.
256 devices in a mesh: sp: 64 (over z, x, core), tp: 4 (over y).
Axes of the slice: x: 4, y: 4, z: 8, core: 2. Of those that a mesh axis runs over, the one named last changes fastest.
Arguments:
- stream_in: bfloat16 [16384, 2048], P(('sp', 'tp')), may hold values from -6 to 6
- queries: bfloat16 [16384, 1024], P('sp', 'tp'), may hold values from -48 to 48
- keys: bfloat16 [16384, 512], P('sp', 'tp'), may hold values from -48 to 48
- values: bfloat16 [16384, 512], P('sp', 'tp'), may hold values from -6 to 6
- query_gain: float32 [64], replicated, may hold values from 1.5 to 6
- key_gain: float32 [64], replicated, may hold values from 1.5 to 6
- out_rows: bfloat16 [1024, 2048], P('tp'), may hold values from -0.1875 to 0.1875
- norm_gain: float32 [2048], replicated, may hold values from 0.1 to 1.9
- route_ids: int32 [16384, 2], P(('sp', 'tp')), may hold values from 0 to 63, all different within a row; in each aligned block of 64 rows (0 to 63, 64 to 127, ...) at most 3 rows name the same one
- route_weights: float32 [16384, 2], P(('sp', 'tp')), may hold values from 0.25 to 1
- gate_weight: bfloat16 [64, 2048, 3072], P('sp', None, 'tp'), may hold values from -0.125 to 0.125
- up_weight: bfloat16 [64, 2048, 3072], P('sp', None, 'tp'), may hold values from -0.125 to 0.125
- down_weight: bfloat16 [64, 3072, 2048], P('sp', 'tp'), may hold values from -0.109375 to 0.109375
Outputs:
- stream_out: bfloat16 [16384, 2048], P(('sp', 'tp'))
Inputs may be any that keep to these rules, and one draw needn't show every extreme that they name: `route_ids`: each row names 2 different experts; among the rows of one device no expert is named more than 3 times.
All inputs are finite; a program needn't handle non-finite values.
Results may differ from a plain program's by a relative error of at most 0.014.
The roundings to bfloat16 on the way count: a program that leaves them out, or rounds other values in their place, can miss the bound.
Values may be sent and summed in bfloat16 or wider, within the bound.
A program may use at most 128 MiB of HBM per device.

v0:
```python
import math
import jax
import jax.numpy as jnp
from jax import lax
from jax.sharding import PartitionSpec as P

GRID_W = 64
EPS = 1e-06
THETA = 10000.0


def partner(x, axis, distance):
    return lax.ppermute(x, axis, [(i, i ^ 1 << distance) for i in range(lax.axis_size(axis))])


def grouped_exchange(x, axis, split_dim, concat_dim, work, item_dim, out_dim):
    items = jax.tree.leaves(x)[0].shape[item_dim]
    count = 2 if items % 2 == 0 else 1
    outs = []
    for k in range(count):
        group = jax.tree.map(
            lambda a: lax.slice_in_dim(
                a, k * (items // count), (k + 1) * (items // count), axis=item_dim
            ),
            x,
        )
        outs.append(
            work(
                lax.all_to_all(
                    group, axis, split_axis=split_dim, concat_axis=concat_dim, tiled=True
                )
            )
        )
    return jax.tree.map(lambda *parts: jnp.concatenate(parts, axis=out_dim), *outs)


def turn_tables(offset, count, head_size):
    position = offset + jnp.arange(count, dtype=jnp.int32)
    grid_row = (position // GRID_W).astype(jnp.float32)
    column = (position % GRID_W).astype(jnp.float32)
    pair_index = jnp.arange(head_size // 4, dtype=jnp.float32)
    inverse = THETA ** (-4.0 * pair_index / head_size)
    angles = jnp.concatenate([grid_row[:, None] * inverse, column[:, None] * inverse], axis=1)
    return (jnp.cos(angles), jnp.sin(angles))


def normalize_rotate(block_data, gain_vector, cos_table, sin_table):
    row_count = block_data.shape[0]
    head_size = gain_vector.shape[0]
    wide = block_data.astype(jnp.float32).reshape(row_count, -1, head_size)
    wide = wide * lax.rsqrt(jnp.mean(wide * wide, axis=-1, keepdims=True) + EPS) * gain_vector
    pairs = wide.reshape(row_count, wide.shape[1], head_size // 2, 2)
    even_part = pairs[..., 0]
    odd_part = pairs[..., 1]
    cosine = cos_table[:, None, :]
    sine_part = sin_table[:, None, :]
    turned = jnp.stack(
        [even_part * cosine - odd_part * sine_part, even_part * sine_part + odd_part * cosine],
        axis=-1,
    )
    return turned.reshape(row_count, -1).astype(jnp.bfloat16)


def local(
    stream_in,
    queries,
    keys,
    values,
    query_gain,
    key_gain,
    out_rows,
    norm_gain,
    route_ids,
    route_weights,
    gate_weight,
    up_weight,
    down_weight,
):
    head_size = query_gain.shape[0]
    seq_rows = queries.shape[0]
    query_heads = queries.shape[1] // head_size
    key_heads = keys.shape[1] // head_size
    group_head_count = query_heads // key_heads
    whole_out = lax.all_gather(out_rows, "tp", axis=0, tiled=True)
    place_in_seq = lax.axis_index("sp")
    cos_table, sin_table = turn_tables(place_in_seq * seq_rows, seq_rows, head_size)
    rotated_queries = normalize_rotate(queries, query_gain, cos_table, sin_table).reshape(
        seq_rows, key_heads, group_head_count, head_size
    )
    rotated_keys = normalize_rotate(keys, key_gain, cos_table, sin_table)
    score_scale = head_size ** (-0.5)

    def absorb(carry, pieces):
        key_piece, value_piece = pieces
        sequence_length = key_piece.shape[0]
        span_rows = math.gcd(sequence_length, 4 * seq_rows)
        block_count = sequence_length // span_rows
        key_blocks = key_piece.reshape(block_count, span_rows, key_heads, head_size)
        value_blocks = value_piece.reshape(block_count, span_rows, key_heads, head_size)

        def one_block(running, blocks_pair):
            row_top, row_total, weighted = running
            key_block, value_block = blocks_pair
            scores = (
                jnp.einsum(
                    "qkgd,skd->qkgs", rotated_queries, key_block, preferred_element_type=jnp.float32
                )
                * score_scale
            )
            new_top = jnp.maximum(row_top, jnp.max(scores, axis=-1))
            weights = jnp.exp(scores - new_top[..., None])
            shrink = jnp.exp(row_top - new_top)
            row_total = row_total * shrink + jnp.sum(weights, axis=-1)
            weighted = weighted * shrink[..., None] + jnp.einsum(
                "qkgs,skd->qkgd",
                weights.astype(jnp.bfloat16),
                value_block,
                preferred_element_type=jnp.float32,
            )
            return ((new_top, row_total, weighted), None)

        return lax.scan(one_block, carry, (key_blocks, value_blocks))[0]

    start_top = jnp.full((seq_rows, key_heads, group_head_count), -1e30, jnp.float32)
    start_total = jnp.zeros((seq_rows, key_heads, group_head_count), jnp.float32)
    start_weighted = jnp.zeros((seq_rows, key_heads, group_head_count, head_size), jnp.float32)
    carried = absorb((start_top, start_total, start_weighted), (rotated_keys, values))
    held_keys = rotated_keys
    held_values = values
    level_count = lax.axis_size("sp").bit_length() - 1
    for bit in range(level_count):
        partner_keys, partner_values = partner((held_keys, held_values), "sp", bit)
        carried = absorb(carried, (partner_keys, partner_values))
        if bit + 1 < level_count:
            held_keys = jnp.concatenate([held_keys, partner_keys], axis=0)
            held_values = jnp.concatenate([held_values, partner_values], axis=0)
    row_top, row_total, weighted = carried
    attended = (
        (weighted / row_total[..., None])
        .astype(jnp.bfloat16)
        .reshape(seq_rows, query_heads * head_size)
    )
    token_heads = lax.all_to_all(attended, "tp", split_axis=0, concat_axis=1, tiled=True)
    projected = jnp.dot(token_heads, whole_out, preferred_element_type=jnp.float32)
    stream = (stream_in.astype(jnp.float32) + projected).astype(jnp.bfloat16)
    stream_wide = stream.astype(jnp.float32)
    normed = (
        stream_wide
        * lax.rsqrt(jnp.mean(stream_wide * stream_wide, axis=1, keepdims=True) + EPS)
        * norm_gain
    ).astype(jnp.bfloat16)
    tokens = stream.shape[0]
    model_width = stream.shape[1]
    top_count = route_ids.shape[1]
    experts = lax.axis_size("sp")
    routed = tokens * top_count
    capacity = max(2, (5 * routed + 4 * experts - 1) // (4 * experts))
    flat_ids = route_ids.reshape(routed)
    member = (flat_ids[:, None] == jnp.arange(experts, dtype=jnp.int32)[None, :]).astype(jnp.int32)
    earlier = jnp.cumsum(member, axis=0) - member
    slot_rank = jnp.sum(earlier * member, axis=1)
    target = flat_ids * capacity + slot_rank
    placed = (target[:, None] == jnp.arange(experts * capacity, dtype=jnp.int32)[None, :]).astype(
        jnp.bfloat16
    )
    placed = placed.reshape(tokens, top_count, experts * capacity)
    outgoing = jnp.einsum("tks,td->sd", placed, normed, preferred_element_type=jnp.float32).astype(
        jnp.bfloat16
    )
    outgoing = outgoing.reshape(experts, capacity, model_width)
    gate_shard = gate_weight[0]
    up_shard = up_weight[0]
    down_shard = down_weight[0]

    def expert_work(arrived):
        sources, slot_count, width_here = arrived.shape
        flat_rows = arrived.reshape(sources * slot_count, width_here)
        row_piece = lax.all_gather(flat_rows, "tp", axis=0, tiled=True)
        gate_value = jnp.dot(row_piece, gate_shard, preferred_element_type=jnp.float32)
        up_value = jnp.dot(row_piece, up_shard, preferred_element_type=jnp.float32)
        hidden = (jax.nn.silu(gate_value) * up_value).astype(jnp.bfloat16)
        summed = lax.psum_scatter(
            jnp.dot(
                lax.slice_in_dim(hidden, 0, sources * slot_count * lax.axis_size("tp"), axis=0),
                down_shard,
                preferred_element_type=jnp.float32,
            ).astype(jnp.bfloat16),
            "tp",
            scatter_dimension=0,
            tiled=True,
        )
        answer = summed.reshape(sources, slot_count, width_here)
        return lax.all_to_all(answer, "sp", split_axis=0, concat_axis=0, tiled=True)

    returned = grouped_exchange(outgoing, "sp", 0, 0, expert_work, 1, 1)
    expert_back = returned.reshape(experts * capacity, model_width)
    picked = jnp.einsum("tks,sd->tkd", placed, expert_back, preferred_element_type=jnp.float32)
    mixed_out = stream_wide + jnp.sum(route_weights[:, :, None] * picked, axis=1)
    return mixed_out.astype(jnp.bfloat16)


def solution(mesh):
    return jax.shard_map(
        local,
        mesh=mesh,
        in_specs=(
            P(("sp", "tp"), None),
            P("sp", "tp"),
            P("sp", "tp"),
            P("sp", "tp"),
            P(),
            P(),
            P("tp", None),
            P(),
            P(("sp", "tp"), None),
            P(("sp", "tp"), None),
            P("sp", None, "tp"),
            P("sp", None, "tp"),
            P("sp", "tp", None),
        ),
        out_specs=P(("sp", "tp"), None),
        check_vma=False,
    )
```

profile of v0, /device:TPU:1, one launch (start us, length us, event | category | flops | bytes accessed | tf_op | source)
XLA Modules:
  0.0 646.2 jit_solution(744757202785638066)
XLA Ops:
  9.6 3.3 collective-permute-start
  23.6 2.3 fusion.122
  41.1 1.9 collective-permute-start.5
  51.2 2.2 pad_maximum_fusion
  56.2 1.9 collective-permute-start.7
  60.5 1.9 constant_dynamic-update-slice_fusion.12
  64.1 3.1 fusion.80
  67.2 2.2 reshape.298
  69.5 2.0 copy.102
  71.5 5.5 collective-permute-done.7
  77.0 3.2 reshape.324
  80.1 3.5 copy.103
  83.7 2.1 constant_dynamic-update-slice_fusion.11
  87.4 2.2 constant_dynamic-update-slice_fusion.17
  90.3 7.3 %while.6 = (s32[]{:T(128)}, f32[256,2,2]{0,2,1:T(2,128)S(1)}, f32[256,2,2]{0,2,1:T(2,128)S(1)}, f32[256,2,2,64]{0,3,2,1:T(8,128)S(1)}, bf16[2,1024,2,64]{1,3,2,0...) while((s32[]{:T(128)}, f32[256,2,2]{0,2,1:T(2,128)S(1)}, ...), condition=%wide.region_13.14_spmd, body=%wide.region_10.13_spmd.sunk | while | flops 276957184 | bytes 15925377 | solution.py:122
  97.6 59.1 %collective-permute-done.8 = bf16[4096,128]{0,1:T(8,128)(2,1)} collective-permute-done((bf16[4096,128]{0,1:T(8,128)(2,1)}, bf16[4096,128]{0,1:T(8,128)(2,1)}, u32[]{:S(2)}, u32[]{:S(2)}) %collective-permute-start.8) | collective-permute-done | bytes 1048608 | tf_op jit(solution)/shard_map/ppermute | solution.py:13
  156.8 2.6 reshape.300
  159.4 2.5 copy.105
  161.9 17.3 %collective-permute-done.9 = bf16[4096,128]{1,0:T(8,128)(2,1)} collective-permute-done((bf16[4096,128]{1,0:T(8,128)(2,1)}, bf16[4096,128]{1,0:T(8,128)(2,1)}, u32[]{:S(2)}, u32[]{:S(2)}) %collective-permute-start.9) | collective-permute-done | bytes 1048608 | tf_op jit(solution)/shard_map/ppermute | solution.py:13
  179.2 5.0 reshape.325
  184.2 5.9 copy.106
  190.1 2.3 constant_dynamic-update-slice_fusion.10
  192.4 5.0 collective-permute-start.10
  197.4 2.3 constant_dynamic-update-slice_fusion.16
  200.2 17.3 %while.7 = (s32[]{:T(128)}, f32[256,2,2]{0,2,1:T(2,128)S(1)}, f32[256,2,2]{0,2,1:T(2,128)S(1)}, f32[256,2,2,64]{0,3,2,1:T(8,128)S(1)}, bf16[4,1024,2,64]{1,3,2,0...) while((s32[]{:T(128)}, f32[256,2,2]{0,2,1:T(2,128)S(1)}, ...), condition=%wide.region_17.18_spmd, body=%wide.region_14.17_spmd.sunk | while | flops 276957184 | bytes 13828197 | solution.py:122
  202.7 1.8 fusion.167
  207.0 1.8 fusion.167
  217.5 94.2 %collective-permute-done.10 = bf16[8192,128]{0,1:T(8,128)(2,1)} collective-permute-done((bf16[8192,128]{0,1:T(8,128)(2,1)}, bf16[8192,128]{0,1:T(8,128)(2,1)}, u32[]{:S(2)}, u32[]{:S(2)}) %collective-permute-start.10) | collective-permute-done | bytes 2097184 | tf_op jit(solution)/shard_map/ppermute | solution.py:13
  311.7 3.0 copy.143
  314.7 2.5 copy.108
  317.2 61.5 %collective-permute-done.11 = bf16[8192,128]{1,0:T(8,128)(2,1)} collective-permute-done((bf16[8192,128]{1,0:T(8,128)(2,1)}, bf16[8192,128]{1,0:T(8,128)(2,1)}, u32[]{:S(2)}, u32[]{:S(2)}) %collective-permute-start.11) | collective-permute-done | bytes 2097184 | tf_op jit(solution)/shard_map/ppermute | solution.py:13
  378.6 8.3 %reshape.326 = bf16[8,1024,2,64]{3,2,1,0:T(2,128)(2,1)} reshape(bf16[8192,128]{1,0:T(8,128)(2,1)} %collective-permute-done.11) | data formatting | bytes 4194304 | tf_op jit(solution)/shard_map/reshape | solution.py:99
  386.9 10.7 %copy.109 = bf16[8,1024,2,64]{1,3,2,0:T(8,128)(2,1)} copy(bf16[8,1024,2,64]{3,2,1,0:T(2,128)(2,1)} %reshape.326) | data formatting | bytes 4194304 | tf_op jit(solution)/shard_map/while | solution.py:122
  397.5 34.5 %while.8 = (s32[]{:T(128)}, f32[256,2,2]{0,2,1:T(2,128)S(1)}, f32[256,2,2]{0,2,1:T(2,128)S(1)}, f32[256,2,2,64]{0,3,2,1:T(8,128)S(1)}, bf16[8,1024,2,64]{1,3,2,0...) while((s32[]{:T(128)}, f32[256,2,2]{0,2,1:T(2,128)S(1)}, ...), condition=%wide.region_21.22_spmd, body=%wide.region_18.21_spmd.sunk | while | flops 276957184 | bytes 13828197 | solution.py:122
  404.3 1.8 fusion.172
  434.7 4.0 all-to-all-start
  438.7 4.7 all-to-all-done
  443.5 3.2 multiply_reduce_fusion
  448.9 3.3 reshape.304
  452.2 38.9 %all_to_all.29 = bf16[64,3,2048]{2,1,0:T(4,128)(2,1)} all-to-all(bf16[64,3,2048]{2,1,0:T(4,128)(2,1)} %reshape.304), channel_id=1, replica_groups=mesh['sp'=64,'tp'=4] {'sp'}, dimensions={0} | all-to-all | bytes 1572864 | tf_op jit(solution)/shard_map/all_to_all | solution.py:29
  491.1 3.2 reshape.305
  494.4 37.1 %all-gather.5.cloned.1.call-done = bf16[768,2048]{1,0:T(8,128)(2,1)} async-done(((bf16[192,2048]{1,0:T(8,128)(2,1)}), bf16[768,2048]{1,0:T(8,128)(2,1)}) %all-gather.5.cloned.1.call-update) | async-done | bytes 3145744 | tf_op jit(solution)/shard_map/all_gather | solution.py:178
  531.4 6.9 %fusion.61 = f32[768,768]{1,0:T(8,128)} fusion(bf16[768,2048]{1,0:T(8,128)(2,1)} %all-gather.5.cloned.1.call-done, bf16[1,2048,768]{2,1,0:T(8,128)(2,1)} %param.30), kind=kOutput, calls=%fused_computation.61 | convolution fusion | flops 2415919104 | bytes 8650752 | tf_op jit(solution)/shard_map/dot_general | solution.py:180
  538.3 11.0 %convolution_convert_fusion = bf16[768,2048]{1,0:T(8,128)(2,1)} fusion(bf16[1,768,2048]{2,1,0:T(8,128)(2,1)S(1)} %copy-done, f32[768,768]{1,0:T(8,128)} %fusion.61, bf16[768,2048]{1,0:T(8,128)(2,1)} %all-gather.5.cloned.1.call-done, bf16[1,2048,768]{2,1,0:T(8,128)(2,1)} %param.29), kind=kOutput, calls=%fused_computation.59 | convolution fusion | flops 4836950016 | bytes 14942208 | tf_op jit(solution)/shard_map/dot_general | solution.py:183
  549.4 41.3 %reduce-scatter.2.cloned.1.call-done = bf16[192,2048]{1,0:T(8,128)(2,1)} async-done(((bf16[768,2048]{1,0:T(8,128)(2,1)}), bf16[192,2048]{1,0:T(8,128)(2,1)}) %reduce-scatter.2.cloned.1.call-update) | async-done | bytes 786448 | tf_op jit(solution)/shard_map/reduce_scatter | solution.py:182
  590.7 3.3 reshape.306
  593.9 39.0 %all_to_all.30 = bf16[64,3,2048]{2,1,0:T(4,128)(2,1)} all-to-all(bf16[64,3,2048]{2,1,0:T(4,128)(2,1)} %reshape.306), channel_id=1, replica_groups=mesh['sp'=64,'tp'=4] {'sp'}, dimensions={0} | all-to-all | bytes 1572864 | tf_op jit(solution)/shard_map/all_to_all | solution.py:193
  632.9 3.2 reshape.322
  (223 shorter events, 107.9 us)
Async XLA Ops:
  6.5 531.8 %copy-start = (bf16[1,768,2048]{2,1,0:T(8,128)(2,1)S(1)}, bf16[1,768,2048]{2,1,0:T(8,128)(2,1)}, u32[]{:S(2)}) copy-start(bf16[1,768,2048]{2,1,0:T(8,128)(2,1)} %param.31) | copy-start | bytes 9437188
  6.5 9.1 %copy-start.12 = (bf16[256,128]{1,0:T(8,128)(2,1)S(1)}, bf16[256,128]{1,0:T(8,128)(2,1)}, u32[]{:S(2)}) copy-start(bf16[256,128]{1,0:T(8,128)(2,1)} %param.22) | copy-start | bytes 196612
  6.5 10.5 %copy-start.24 = (f32[64]{0:T(128)S(1)}, f32[64]{0:T(128)}, u32[]{:S(2)}) copy-start(f32[64]{0:T(128)} %param.23) | copy-start | bytes 772
  6.5 14.7 %copy-start.22 = (s32[64,2]{0,1:T(2,128)S(1)}, s32[64,2]{0,1:T(2,128)}, u32[]{:S(2)}) copy-start(s32[64,2]{0,1:T(2,128)} %param.27) | copy-start | bytes 1540
  6.5 437.0 %all-gather.3.cloned.1.call-start = ((), (), s32[]{:S(2)}) async-start(), calls=%async_computation.4 | async-start | bytes 5242880 | tf_op jit(solution)/shard_map/all_gather | solution.py:84
  8.8 0.6 copy-start.17
  8.8 0.6 copy-start.18
  9.6 16.9 %copy-start.14 = (bf16[256,128]{0,1:T(8,128)(2,1)}, bf16[256,128]{0,1:T(8,128)(2,1)S(1)}, u32[]{:S(2)}) copy-start(bf16[256,128]{0,1:T(8,128)(2,1)S(1)} %convert_element_type.105) | copy-start | bytes 196612
  9.6 16.9 %collective-permute-start = (bf16[256,128]{0,1:T(8,128)(2,1)S(1)}, bf16[256,128]{0,1:T(8,128)(2,1)S(1)}, u32[]{:S(2)}, u32[]{:S(2)}) collective-permute-start(bf16[256,128]{0,1:T(8,128)(2,1)S(1)} %convert_element_type.105), channel_id=1, source_target_pairs={{0,4},{4,0},{8,12},{12,8},{16,20},{20,16},{24,28},{28,24},{32,36},... | collective-permute-start | bytes 196616 | tf_op jit(solution)/shard_map/ppermute | solution.py:13
  12.9 15.6 %collective-permute-start.3 = (bf16[256,128]{1,0:T(8,128)(2,1)}, bf16[256,128]{1,0:T(8,128)(2,1)}, u32[]{:S(2)}, u32[]{:S(2)}) collective-permute-start(bf16[256,128]{1,0:T(8,128)(2,1)} %param.22), channel_id=1, source_target_pairs={{0,4},{4,0},{8,12},{12,8},{16,20},{20,16},{24,28},{28,24},{32,36},... | collective-permute-start | bytes 196616 | tf_op jit(solution)/shard_map/ppermute | solution.py:13
  26.6 2.0 copy-start.10
  27.2 8.9 %collective-permute-start.1 = (bf16[512,128]{0,1:T(8,128)(2,1)}, bf16[512,128]{0,1:T(8,128)(2,1)S(1)}, u32[]{:S(2)}, u32[]{:S(2)}) collective-permute-start(bf16[512,128]{0,1:T(8,128)(2,1)} %pad_maximum_fusion.5), channel_id=1, source_target_pairs={{0,8},{4,12},{8,0},{12,4},{16,24},{20,28},{24,16},{28,20},{32,40},... | collective-permute-start | bytes 393224 | tf_op jit(solution)/shard_map/ppermute | solution.py:13
  30.1 8.8 %collective-permute-start.4 = (bf16[512,128]{1,0:T(8,128)(2,1)}, bf16[512,128]{1,0:T(8,128)(2,1)S(1)}, u32[]{:S(2)}, u32[]{:S(2)}) collective-permute-start(bf16[512,128]{1,0:T(8,128)(2,1)} %pad_maximum_fusion.6), channel_id=1, source_target_pairs={{0,8},{4,12},{8,0},{12,4},{16,24},{20,28},{24,16},{28,20},{32,40},... | collective-permute-start | bytes 393224 | tf_op jit(solution)/shard_map/ppermute | solution.py:13
  36.1 2.7 copy-start.6
  37.8 11.6 %collective-permute-start.2 = (bf16[1024,128]{0,1:T(8,128)(2,1)}, bf16[1024,128]{0,1:T(8,128)(2,1)}, u32[]{:S(2)}, u32[]{:S(2)}) collective-permute-start(bf16[1024,128]{0,1:T(8,128)(2,1)} %pad_maximum_fusion.2), channel_id=1, source_target_pairs={{0,16},{4,20},{8,24},{12,28},{16,0},{20,4},{24,8},{28,12},{32,48},... | collective-permute-start | bytes 786440 | tf_op jit(solution)/shard_map/ppermute | solution.py:13
  38.8 0.7 copy-start.8
  41.1 13.3 %collective-permute-start.5 = (bf16[1024,128]{1,0:T(8,128)(2,1)}, bf16[1024,128]{1,0:T(8,128)(2,1)S(1)}, u32[]{:S(2)}, u32[]{:S(2)}) collective-permute-start(bf16[1024,128]{1,0:T(8,128)(2,1)} %pad_maximum_fusion.3), channel_id=1, source_target_pairs={{0,16},{4,20},{8,24},{12,28},{16,0},{20,4},{24,8},{28,12},{32,48},... | collective-permute-start | bytes 786440 | tf_op jit(solution)/shard_map/ppermute | solution.py:13
  47.9 3.3 copy-start.7
  47.9 3.3 copy-start.11
  47.9 3.3 copy-start.15
  49.4 4.4 copy-start.16
  51.2 6.9 %copy-start.1 = (f32[2,1024,256,2]{2,1,3,0:T(8,128)}, f32[2,1024,256,2]{2,1,3,0:T(8,128)S(1)}, u32[]{:S(2)}) copy-start(f32[2,1024,256,2]{2,1,3,0:T(8,128)S(1)} %get-tuple-element.368) | copy-start | bytes 12582916
  51.2 3.1 copy-start.9
  51.2 3.1 copy-start.13
  53.4 13.8 %collective-permute-start.6 = (bf16[2048,128]{0,1:T(8,128)(2,1)}, bf16[2048,128]{0,1:T(8,128)(2,1)}, u32[]{:S(2)}, u32[]{:S(2)}) collective-permute-start(bf16[2048,128]{0,1:T(8,128)(2,1)} %pad_maximum_fusion), channel_id=1, source_target_pairs={{0,32},{4,36},{8,40},{12,44},{16,48},{20,52},{24,56},{28,60},{32,0... | collective-permute-start | bytes 1572872 | tf_op jit(solution)/shard_map/ppermute | solution.py:13
  54.3 4.5 copy-start.3
  54.3 4.6 copy-start.2
  56.2 20.8 %collective-permute-start.7 = (bf16[2048,128]{1,0:T(8,128)(2,1)}, bf16[2048,128]{1,0:T(8,128)(2,1)}, u32[]{:S(2)}, u32[]{:S(2)}) collective-permute-start(bf16[2048,128]{1,0:T(8,128)(2,1)} %pad_maximum_fusion.1), channel_id=1, source_target_pairs={{0,32},{4,36},{8,40},{12,44},{16,48},{20,52},{24,56},{28,60},{32,0... | collective-permute-start | bytes 1572872 | tf_op jit(solution)/shard_map/ppermute | solution.py:13
  58.1 1.1 copy-start.19
  58.1 1.4 copy-start.20
  85.8 71.0 %collective-permute-start.8 = (bf16[4096,128]{0,1:T(8,128)(2,1)}, bf16[4096,128]{0,1:T(8,128)(2,1)}, u32[]{:S(2)}, u32[]{:S(2)}) collective-permute-start(bf16[4096,128]{0,1:T(8,128)(2,1)} %get-tuple-element.340), channel_id=1, source_target_pairs={{0,64},{4,68},{8,72},{12,76},{16,80},{20,84},{24,88},{28,92},{32,9... | collective-permute-start | bytes 3145736 | tf_op jit(solution)/shard_map/ppermute | solution.py:13
  89.6 89.7 %collective-permute-start.9 = (bf16[4096,128]{1,0:T(8,128)(2,1)}, bf16[4096,128]{1,0:T(8,128)(2,1)}, u32[]{:S(2)}, u32[]{:S(2)}) collective-permute-start(bf16[4096,128]{1,0:T(8,128)(2,1)} %get-tuple-element.338), channel_id=1, source_target_pairs={{0,64},{4,68},{8,72},{12,76},{16,80},{20,84},{24,88},{28,92},{32,9... | collective-permute-start | bytes 3145736 | tf_op jit(solution)/shard_map/ppermute | solution.py:13
  92.1 1.0 copy-start.4
  95.7 1.0 copy-start.4
  192.4 119.3 %collective-permute-start.10 = (bf16[8192,128]{0,1:T(8,128)(2,1)}, bf16[8192,128]{0,1:T(8,128)(2,1)}, u32[]{:S(2)}, u32[]{:S(2)}) collective-permute-start(bf16[8192,128]{0,1:T(8,128)(2,1)} %constant_dynamic-update-slice_fusion.10), channel_id=1, source_target_pairs={{0,128},{4,132},{8,136},{12,140},{16,144},{20,148},{24,152},{28,15... | collective-permute-start | bytes 6291464 | tf_op jit(solution)/shard_map/ppermute | solution.py:13
  199.7 178.9 %collective-permute-start.11 = (bf16[8192,128]{1,0:T(8,128)(2,1)}, bf16[8192,128]{1,0:T(8,128)(2,1)}, u32[]{:S(2)}, u32[]{:S(2)}) collective-permute-start(bf16[8192,128]{1,0:T(8,128)(2,1)} %constant_dynamic-update-slice_fusion.16), channel_id=1, source_target_pairs={{0,128},{4,132},{8,136},{12,140},{16,144},{20,148},{24,152},{28,15... | collective-permute-start | bytes 6291464 | tf_op jit(solution)/shard_map/ppermute | solution.py:13
  432.8 14.8 %copy-start.21 = (f32[2048]{0:T(1024)S(1)}, f32[2048]{0:T(1024)}, u32[]{:S(2)}) copy-start(f32[2048]{0:T(1024)} %param.26) | copy-start | bytes 24580
  434.7 8.8 %all-to-all-start = ((bf16[4,64,256]{2,1,0:T(8,128)(2,1)}), bf16[4,64,256]{2,1,0:T(8,128)(2,1)S(1)}, u32[]{:S(2)}, u32[]{:S(2)}) async-start(bf16[4,64,256]{2,1,0:T(8,128)(2,1)} %copy.141), calls=%async_computation | async-start | bytes 262144 | tf_op jit(solution)/shard_map/all_to_all | solution.py:143
  438.6 92.8 %all-gather.5.cloned.1.call-start = ((), (), s32[]{:S(2)}) async-start(), calls=%async_computation.5 | async-start | bytes 3932160 | tf_op jit(solution)/shard_map/all_gather | solution.py:178
  446.7 0.9 copy-start.5
  494.3 96.3 %reduce-scatter.2.cloned.1.call-start = ((), (), s32[]{:S(2)}) async-start(), calls=%async_computation.6 | async-start | bytes 3932160 | tf_op jit(solution)/shard_map/reduce_scatter | solution.py:182
  549.4 86.8 %copy-start.23 = (f32[64,2]{0,1:T(2,128)S(1)}, f32[64,2]{0,1:T(2,128)}, u32[]{:S(2)}) copy-start(f32[64,2]{0,1:T(2,128)} %param.28) | copy-start | bytes 1540
Sparse Core Ops, SparseCore 0:
  13.2 51.5 all-gather.2
  494.4 36.9 all-gather.4
  549.5 41.1 reduce-scatter.1
where the time goes:
time: 657 us; the launch traced here: 646 us
  waiting for transfers between devices  321 us (49%)
  local copies, waits for them, and re-layouts  98.7 us (15%)
  matrix products  83.3 us (13%)
  blocking collectives  77.9 us (12%)
  other arithmetic  29.4 us (4%)
  starting transfers between devices  21.7 us (3%)
  between operations  13.8 us (2%)
    ppermute x12, waiting for transfers between devices, partner(): lax.ppermute(x, axis, [(i, i ^ 1 << distance) for i in range(lax.axis_siz...  238 us
    reduce_scatter x1, waiting for transfers between devices, expert_work(): lax.psum_scatter(jnp.dot(lax.slice_in_dim(hidden, 0, sources * slot_count...  41.3 us
    all_to_all x1, blocking collectives, expert_work(): return lax.all_to_all(answer, 'sp', split_axis=0, concat_axis=0, tiled=True)  39 us
    all_to_all x1, blocking collectives, grouped_exchange(): lax.all_to_all(group, axis, split_axis=split_dim, concat_axis=concat_dim,...  38.9 us
    all_gather x1, waiting for transfers between devices, expert_work(): row_piece = lax.all_gather(flat_rows, 'tp', axis=0, tiled=True)  37.1 us
    dot_general x18, matrix products, one_block(): jnp.einsum('qkgd,skd->qkgs', rotated_queries, key_block, preferred_elemen...  30.8 us
    dot_general x18, matrix products, one_block(): jnp.einsum('qkgs,skd->qkgd', weights.astype(jnp.bfloat16), value_block, p...  28.5 us
    while x6, local copies, waits for them, and re-layouts, absorb(): return lax.scan(one_block, carry, (key_blocks, value_blocks))[0]  27.1 us
  transfers between devices with their start and end apart: 16, of which 8 were waited for; matrix products, arithmetic and copies ran while one was open for 26% of the time, Pallas kernels for 0%

commit v1 on v0

--- a/solution.py
+++ b/solution.py
@@ -175,7 +175,10 @@
     def expert_work(arrived):
         sources, slot_count, width_here = arrived.shape
         flat_rows = arrived.reshape(sources * slot_count, width_here)
-        row_piece = lax.all_gather(flat_rows, "tp", axis=0, tiled=True)
+        row_piece = jnp.concatenate(
+            lax.all_to_all(jnp.stack([flat_rows for _ in range(lax.psum(1, "tp"))], 0), "tp", 0, 0),
+            axis=0,
+        )
         gate_value = jnp.dot(row_piece, gate_shard, preferred_element_type=jnp.float32)
         up_value = jnp.dot(row_piece, up_shard, preferred_element_type=jnp.float32)
         hidden = (jax.nn.silu(gate_value) * up_value).astype(jnp.bfloat16)

time: 657 us -> 656 us (level)
  waiting for transfers between devices: 321 us -> 280 us
  blocking collectives: 77.9 us -> 117 us
    all_to_all x0 -> x1, blocking collectives: none -> 39.3 us  [expert_work(): lax.all_to_all(jnp.stack([flat_rows for _ in range(lax.psum(1, 'tp'))], 0...]
    all_gather x1 -> x0, waiting for transfers between devices: 37.1 us -> none  [expert_work(): row_piece = lax.all_gather(flat_rows, 'tp', axis=0, tiled=True)]
    unnamed x63 -> x67, local copies, waits for them, and re-layouts: 22.5 us -> 24.3 us
  transfers between devices with their start and end apart: 16 -> 15, of which waited for: 8 -> 7; matrix products, arithmetic and copies ran while one was open for 26% -> 26% of each run, Pallas kernels for 0% -> 0%
where the time goes in v1:
time: 656 us; the launch traced here: 645 us
  waiting for transfers between devices  280 us (43%)
  blocking collectives  117 us (18%)
  local copies, waits for them, and re-layouts  102 us (16%)
  matrix products  80.5 us (12%)
  other arithmetic  29.3 us (4%)
  starting transfers between devices  21.6 us (3%)
  between operations  14.1 us (2%)
    ppermute x12, waiting for transfers between devices, partner(): lax.ppermute(x, axis, [(i, i ^ 1 << distance) for i in range(lax.axis_siz...  238 us
    all_to_all x1, blocking collectives, expert_work(): lax.all_to_all(jnp.stack([flat_rows for _ in range(lax.psum(1, 'tp'))], 0...  39.3 us
    all_to_all x1, blocking collectives, expert_work(): return lax.all_to_all(answer, 'sp', split_axis=0, concat_axis=0, tiled=True)  39 us
    all_to_all x1, blocking collectives, grouped_exchange(): lax.all_to_all(group, axis, split_axis=split_dim, concat_axis=concat_dim,...  38.9 us
    reduce_scatter x1, waiting for transfers between devices, expert_work(): lax.psum_scatter(jnp.dot(lax.slice_in_dim(hidden, 0, sources * slot_count...  37.1 us
    dot_general x18, matrix products, one_block(): jnp.einsum('qkgd,skd->qkgs', rotated_queries, key_block, preferred_elemen...  30.8 us
    dot_general x18, matrix products, one_block(): jnp.einsum('qkgs,skd->qkgd', weights.astype(jnp.bfloat16), value_block, p...  28.5 us
    while x6, local copies, waits for them, and re-layouts, absorb(): return lax.scan(one_block, carry, (key_blocks, value_blocks))[0]  27.1 us
  transfers between devices with their start and end apart: 15, of which 7 were waited for; matrix products, arithmetic and copies ran while one was open for 26% of the time, Pallas kernels for 0%

profile of v1, /device:TPU:1, one launch (start us, length us, event | category | flops | bytes accessed | tf_op | source)
XLA Modules:
  0.0 645.0 jit_solution(7743335574818011838)
XLA Ops:
  9.7 3.3 collective-permute-start
  23.6 2.3 fusion.122
  41.1 1.9 collective-permute-start.5
  51.3 2.2 pad_maximum_fusion
  56.2 1.9 collective-permute-start.7
  60.5 1.9 constant_dynamic-update-slice_fusion.12
  64.2 3.1 fusion.80
  67.3 2.2 reshape.300
  69.5 2.0 copy.102
  71.5 5.5 collective-permute-done.7
  77.0 3.2 reshape.326
  80.2 3.5 copy.103
  83.7 2.2 constant_dynamic-update-slice_fusion.11
  87.5 2.2 constant_dynamic-update-slice_fusion.17
  90.5 7.3 %while.6 = (s32[]{:T(128)}, f32[256,2,2]{0,2,1:T(2,128)S(1)}, f32[256,2,2]{0,2,1:T(2,128)S(1)}, f32[256,2,2,64]{0,3,2,1:T(8,128)S(1)}, bf16[2,1024,2,64]{1,3,2,0...) while((s32[]{:T(128)}, f32[256,2,2]{0,2,1:T(2,128)S(1)}, ...), condition=%wide.region_13.14_spmd, body=%wide.region_10.13_spmd.sunk | while | flops 276957184 | bytes 15925377 | solution.py:122
  97.8 59.1 %collective-permute-done.8 = bf16[4096,128]{0,1:T(8,128)(2,1)} collective-permute-done((bf16[4096,128]{0,1:T(8,128)(2,1)}, bf16[4096,128]{0,1:T(8,128)(2,1)}, u32[]{:S(2)}, u32[]{:S(2)}) %collective-permute-start.8) | collective-permute-done | bytes 1048608 | tf_op jit(solution)/shard_map/ppermute | solution.py:13
  156.9 2.6 reshape.302
  159.6 2.5 copy.105
  162.1 17.3 %collective-permute-done.9 = bf16[4096,128]{1,0:T(8,128)(2,1)} collective-permute-done((bf16[4096,128]{1,0:T(8,128)(2,1)}, bf16[4096,128]{1,0:T(8,128)(2,1)}, u32[]{:S(2)}, u32[]{:S(2)}) %collective-permute-start.9) | collective-permute-done | bytes 1048608 | tf_op jit(solution)/shard_map/ppermute | solution.py:13
  179.4 5.0 reshape.327
  184.4 5.9 copy.106
  190.3 2.4 constant_dynamic-update-slice_fusion.10
  192.6 5.0 collective-permute-start.10
  197.6 2.3 constant_dynamic-update-slice_fusion.16
  200.4 17.3 %while.7 = (s32[]{:T(128)}, f32[256,2,2]{0,2,1:T(2,128)S(1)}, f32[256,2,2]{0,2,1:T(2,128)S(1)}, f32[256,2,2,64]{0,3,2,1:T(8,128)S(1)}, bf16[4,1024,2,64]{1,3,2,0...) while((s32[]{:T(128)}, f32[256,2,2]{0,2,1:T(2,128)S(1)}, ...), condition=%wide.region_17.18_spmd, body=%wide.region_14.17_spmd.sunk | while | flops 276957184 | bytes 13828197 | solution.py:122
  202.9 1.8 fusion.167
  207.2 1.8 fusion.167
  217.7 94.5 %collective-permute-done.10 = bf16[8192,128]{0,1:T(8,128)(2,1)} collective-permute-done((bf16[8192,128]{0,1:T(8,128)(2,1)}, bf16[8192,128]{0,1:T(8,128)(2,1)}, u32[]{:S(2)}, u32[]{:S(2)}) %collective-permute-start.10) | collective-permute-done | bytes 2097184 | tf_op jit(solution)/shard_map/ppermute | solution.py:13
  312.2 3.0 copy.143
  315.2 2.5 copy.108
  317.7 61.1 %collective-permute-done.11 = bf16[8192,128]{1,0:T(8,128)(2,1)} collective-permute-done((bf16[8192,128]{1,0:T(8,128)(2,1)}, bf16[8192,128]{1,0:T(8,128)(2,1)}, u32[]{:S(2)}, u32[]{:S(2)}) %collective-permute-start.11) | collective-permute-done | bytes 2097184 | tf_op jit(solution)/shard_map/ppermute | solution.py:13
  378.9 8.3 %reshape.328 = bf16[8,1024,2,64]{3,2,1,0:T(2,128)(2,1)} reshape(bf16[8192,128]{1,0:T(8,128)(2,1)} %collective-permute-done.11) | data formatting | bytes 4194304 | tf_op jit(solution)/shard_map/reshape | solution.py:99
  387.1 10.6 %copy.109 = bf16[8,1024,2,64]{1,3,2,0:T(8,128)(2,1)} copy(bf16[8,1024,2,64]{3,2,1,0:T(2,128)(2,1)} %reshape.328) | data formatting | bytes 4194304 | tf_op jit(solution)/shard_map/while | solution.py:122
  397.8 34.5 %while.8 = (s32[]{:T(128)}, f32[256,2,2]{0,2,1:T(2,128)S(1)}, f32[256,2,2]{0,2,1:T(2,128)S(1)}, f32[256,2,2,64]{0,3,2,1:T(8,128)S(1)}, bf16[8,1024,2,64]{1,3,2,0...) while((s32[]{:T(128)}, f32[256,2,2]{0,2,1:T(2,128)S(1)}, ...), condition=%wide.region_21.22_spmd, body=%wide.region_18.21_spmd.sunk | while | flops 276957184 | bytes 13828197 | solution.py:122
  400.2 1.8 fusion.172
  434.9 3.9 all-to-all-start
  438.9 4.7 all-to-all-done
  443.7 3.2 multiply_reduce_fusion
  449.1 3.3 reshape.306
  452.4 38.9 %all_to_all.34 = bf16[64,3,2048]{2,1,0:T(4,128)(2,1)} all-to-all(bf16[64,3,2048]{2,1,0:T(4,128)(2,1)} %reshape.306), channel_id=1, replica_groups=mesh['sp'=64,'tp'=4] {'sp'}, dimensions={0} | all-to-all | bytes 1572864 | tf_op jit(solution)/shard_map/all_to_all | solution.py:29
  491.3 3.2 stack_reshape.2
  496.0 39.3 %all_to_all.35 = bf16[4,192,2048]{2,1,0:T(8,128)(2,1)S(1)} all-to-all(bf16[4,192,2048]{2,1,0:T(8,128)(2,1)S(1)} %stack.16), channel_id=1, replica_groups=mesh['sp'=64,'tp'=4] {'tp'}, dimensions={0} | all-to-all | bytes 6291456 | tf_op jit(solution)/shard_map/all_to_all | solution.py:179
  537.0 4.1 fusion.61
  541.1 11.0 %convolution_convert_fusion = bf16[768,2048]{1,0:T(8,128)(2,1)} fusion(bf16[1,768,2048]{2,1,0:T(8,128)(2,1)S(1)} %copy-done, f32[768,768]{1,0:T(8,128)} %fusion.61, bf16[768,2048]{1,0:T(8,128)(2,1)} %bitcast.297, bf16[1,2048,768]{2,1,0:T(8,128)(2,1)} %param.29), kind=kOutput, calls=%fused_computation.59 | convolution fusion | flops 4836950016 | bytes 14942208 | tf_op jit(solution)/shard_map/dot_general | solution.py:186
  552.1 37.1 %reduce-scatter.2.cloned.1.call-done = bf16[192,2048]{1,0:T(8,128)(2,1)} async-done(((bf16[768,2048]{1,0:T(8,128)(2,1)}), bf16[192,2048]{1,0:T(8,128)(2,1)}) %reduce-scatter.2.cloned.1.call-update) | async-done | bytes 786448 | tf_op jit(solution)/shard_map/reduce_scatter | solution.py:185
  589.2 3.3 reshape.308
  592.5 39.0 %all_to_all.36 = bf16[64,3,2048]{2,1,0:T(4,128)(2,1)} all-to-all(bf16[64,3,2048]{2,1,0:T(4,128)(2,1)} %reshape.308), channel_id=1, replica_groups=mesh['sp'=64,'tp'=4] {'sp'}, dimensions={0} | all-to-all | bytes 1572864 | tf_op jit(solution)/shard_map/all_to_all | solution.py:196
  631.5 3.2 reshape.324
  (226 shorter events, 111.1 us)
Async XLA Ops:
  6.5 534.6 %copy-start = (bf16[1,768,2048]{2,1,0:T(8,128)(2,1)S(1)}, bf16[1,768,2048]{2,1,0:T(8,128)(2,1)}, u32[]{:S(2)}) copy-start(bf16[1,768,2048]{2,1,0:T(8,128)(2,1)} %param.31) | copy-start | bytes 9437188
  6.5 9.1 %copy-start.13 = (bf16[256,128]{1,0:T(8,128)(2,1)S(1)}, bf16[256,128]{1,0:T(8,128)(2,1)}, u32[]{:S(2)}) copy-start(bf16[256,128]{1,0:T(8,128)(2,1)} %param.22) | copy-start | bytes 196612
  6.5 10.5 %copy-start.25 = (f32[64]{0:T(128)S(1)}, f32[64]{0:T(128)}, u32[]{:S(2)}) copy-start(f32[64]{0:T(128)} %param.23) | copy-start | bytes 772
  6.5 14.7 %copy-start.23 = (s32[64,2]{0,1:T(2,128)S(1)}, s32[64,2]{0,1:T(2,128)}, u32[]{:S(2)}) copy-start(s32[64,2]{0,1:T(2,128)} %param.27) | copy-start | bytes 1540
  6.5 437.1 %all-gather.2.cloned.1.call-start = ((), (), s32[]{:S(2)}) async-start(), calls=%async_computation.5 | async-start | bytes 5242880 | tf_op jit(solution)/shard_map/all_gather | solution.py:84
  8.8 0.6 copy-start.18
  8.8 0.6 copy-start.19
  9.6 16.9 %copy-start.15 = (bf16[256,128]{0,1:T(8,128)(2,1)}, bf16[256,128]{0,1:T(8,128)(2,1)S(1)}, u32[]{:S(2)}) copy-start(bf16[256,128]{0,1:T(8,128)(2,1)S(1)} %convert_element_type.105) | copy-start | bytes 196612
  9.7 16.9 %collective-permute-start = (bf16[256,128]{0,1:T(8,128)(2,1)S(1)}, bf16[256,128]{0,1:T(8,128)(2,1)S(1)}, u32[]{:S(2)}, u32[]{:S(2)}) collective-permute-start(bf16[256,128]{0,1:T(8,128)(2,1)S(1)} %convert_element_type.105), channel_id=1, source_target_pairs={{0,4},{4,0},{8,12},{12,8},{16,20},{20,16},{24,28},{28,24},{32,36},... | collective-permute-start | bytes 196616 | tf_op jit(solution)/shard_map/ppermute | solution.py:13
  12.9 15.6 %collective-permute-start.3 = (bf16[256,128]{1,0:T(8,128)(2,1)}, bf16[256,128]{1,0:T(8,128)(2,1)}, u32[]{:S(2)}, u32[]{:S(2)}) collective-permute-start(bf16[256,128]{1,0:T(8,128)(2,1)} %param.22), channel_id=1, source_target_pairs={{0,4},{4,0},{8,12},{12,8},{16,20},{20,16},{24,28},{28,24},{32,36},... | collective-permute-start | bytes 196616 | tf_op jit(solution)/shard_map/ppermute | solution.py:13
  26.6 2.0 copy-start.11
  27.3 8.9 %collective-permute-start.1 = (bf16[512,128]{0,1:T(8,128)(2,1)}, bf16[512,128]{0,1:T(8,128)(2,1)S(1)}, u32[]{:S(2)}, u32[]{:S(2)}) collective-permute-start(bf16[512,128]{0,1:T(8,128)(2,1)} %pad_maximum_fusion.5), channel_id=1, source_target_pairs={{0,8},{4,12},{8,0},{12,4},{16,24},{20,28},{24,16},{28,20},{32,40},... | collective-permute-start | bytes 393224 | tf_op jit(solution)/shard_map/ppermute | solution.py:13
  30.1 8.8 %collective-permute-start.4 = (bf16[512,128]{1,0:T(8,128)(2,1)}, bf16[512,128]{1,0:T(8,128)(2,1)S(1)}, u32[]{:S(2)}, u32[]{:S(2)}) collective-permute-start(bf16[512,128]{1,0:T(8,128)(2,1)} %pad_maximum_fusion.6), channel_id=1, source_target_pairs={{0,8},{4,12},{8,0},{12,4},{16,24},{20,28},{24,16},{28,20},{32,40},... | collective-permute-start | bytes 393224 | tf_op jit(solution)/shard_map/ppermute | solution.py:13
  36.2 2.7 copy-start.7
  37.8 11.6 %collective-permute-start.2 = (bf16[1024,128]{0,1:T(8,128)(2,1)}, bf16[1024,128]{0,1:T(8,128)(2,1)}, u32[]{:S(2)}, u32[]{:S(2)}) collective-permute-start(bf16[1024,128]{0,1:T(8,128)(2,1)} %pad_maximum_fusion.2), channel_id=1, source_target_pairs={{0,16},{4,20},{8,24},{12,28},{16,0},{20,4},{24,8},{28,12},{32,48},... | collective-permute-start | bytes 786440 | tf_op jit(solution)/shard_map/ppermute | solution.py:13
  38.8 0.7 copy-start.9
  41.1 13.3 %collective-permute-start.5 = (bf16[1024,128]{1,0:T(8,128)(2,1)}, bf16[1024,128]{1,0:T(8,128)(2,1)S(1)}, u32[]{:S(2)}, u32[]{:S(2)}) collective-permute-start(bf16[1024,128]{1,0:T(8,128)(2,1)} %pad_maximum_fusion.3), channel_id=1, source_target_pairs={{0,16},{4,20},{8,24},{12,28},{16,0},{20,4},{24,8},{28,12},{32,48},... | collective-permute-start | bytes 786440 | tf_op jit(solution)/shard_map/ppermute | solution.py:13
  48.0 3.3 copy-start.8
  48.0 3.3 copy-start.12
  48.0 3.3 copy-start.16
  49.5 4.4 copy-start.17
  51.2 6.9 %copy-start.1 = (f32[2,1024,256,2]{2,1,3,0:T(8,128)}, f32[2,1024,256,2]{2,1,3,0:T(8,128)S(1)}, u32[]{:S(2)}) copy-start(f32[2,1024,256,2]{2,1,3,0:T(8,128)S(1)} %get-tuple-element.368) | copy-start | bytes 12582916
  51.3 3.1 copy-start.10
  51.3 3.1 copy-start.14
  53.5 13.8 %collective-permute-start.6 = (bf16[2048,128]{0,1:T(8,128)(2,1)}, bf16[2048,128]{0,1:T(8,128)(2,1)}, u32[]{:S(2)}, u32[]{:S(2)}) collective-permute-start(bf16[2048,128]{0,1:T(8,128)(2,1)} %pad_maximum_fusion), channel_id=1, source_target_pairs={{0,32},{4,36},{8,40},{12,44},{16,48},{20,52},{24,56},{28,60},{32,0... | collective-permute-start | bytes 1572872 | tf_op jit(solution)/shard_map/ppermute | solution.py:13
  54.4 4.5 copy-start.3
  54.4 4.7 copy-start.2
  56.2 20.8 %collective-permute-start.7 = (bf16[2048,128]{1,0:T(8,128)(2,1)}, bf16[2048,128]{1,0:T(8,128)(2,1)}, u32[]{:S(2)}, u32[]{:S(2)}) collective-permute-start(bf16[2048,128]{1,0:T(8,128)(2,1)} %pad_maximum_fusion.1), channel_id=1, source_target_pairs={{0,32},{4,36},{8,40},{12,44},{16,48},{20,52},{24,56},{28,60},{32,0... | collective-permute-start | bytes 1572872 | tf_op jit(solution)/shard_map/ppermute | solution.py:13
  58.1 1.1 copy-start.20
  58.1 1.4 copy-start.21
  85.9 71.0 %collective-permute-start.8 = (bf16[4096,128]{0,1:T(8,128)(2,1)}, bf16[4096,128]{0,1:T(8,128)(2,1)}, u32[]{:S(2)}, u32[]{:S(2)}) collective-permute-start(bf16[4096,128]{0,1:T(8,128)(2,1)} %get-tuple-element.340), channel_id=1, source_target_pairs={{0,64},{4,68},{8,72},{12,76},{16,80},{20,84},{24,88},{28,92},{32,9... | collective-permute-start | bytes 3145736 | tf_op jit(solution)/shard_map/ppermute | solution.py:13
  89.7 89.7 %collective-permute-start.9 = (bf16[4096,128]{1,0:T(8,128)(2,1)}, bf16[4096,128]{1,0:T(8,128)(2,1)}, u32[]{:S(2)}, u32[]{:S(2)}) collective-permute-start(bf16[4096,128]{1,0:T(8,128)(2,1)} %get-tuple-element.338), channel_id=1, source_target_pairs={{0,64},{4,68},{8,72},{12,76},{16,80},{20,84},{24,88},{28,92},{32,9... | collective-permute-start | bytes 3145736 | tf_op jit(solution)/shard_map/ppermute | solution.py:13
  92.2 1.0 copy-start.4
  95.9 1.0 copy-start.4
  192.6 119.6 %collective-permute-start.10 = (bf16[8192,128]{0,1:T(8,128)(2,1)}, bf16[8192,128]{0,1:T(8,128)(2,1)}, u32[]{:S(2)}, u32[]{:S(2)}) collective-permute-start(bf16[8192,128]{0,1:T(8,128)(2,1)} %constant_dynamic-update-slice_fusion.10), channel_id=1, source_target_pairs={{0,128},{4,132},{8,136},{12,140},{16,144},{20,148},{24,152},{28,15... | collective-permute-start | bytes 6291464 | tf_op jit(solution)/shard_map/ppermute | solution.py:13
  199.9 178.9 %collective-permute-start.11 = (bf16[8192,128]{1,0:T(8,128)(2,1)}, bf16[8192,128]{1,0:T(8,128)(2,1)}, u32[]{:S(2)}, u32[]{:S(2)}) collective-permute-start(bf16[8192,128]{1,0:T(8,128)(2,1)} %constant_dynamic-update-slice_fusion.16), channel_id=1, source_target_pairs={{0,128},{4,132},{8,136},{12,140},{16,144},{20,148},{24,152},{28,15... | collective-permute-start | bytes 6291464 | tf_op jit(solution)/shard_map/ppermute | solution.py:13
  433.0 14.7 %copy-start.22 = (f32[2048]{0:T(1024)S(1)}, f32[2048]{0:T(1024)}, u32[]{:S(2)}) copy-start(f32[2048]{0:T(1024)} %param.26) | copy-start | bytes 24580
  434.9 8.7 %all-to-all-start = ((bf16[4,64,256]{2,1,0:T(8,128)(2,1)}), bf16[4,64,256]{2,1,0:T(8,128)(2,1)S(1)}, u32[]{:S(2)}, u32[]{:S(2)}) async-start(bf16[4,64,256]{2,1,0:T(8,128)(2,1)} %copy.141), calls=%async_computation | async-start | bytes 262144 | tf_op jit(solution)/shard_map/all_to_all | solution.py:143
  438.8 150.4 %reduce-scatter.2.cloned.1.call-start = ((), (), s32[]{:S(2)}) async-start(), calls=%async_computation.6 | async-start | bytes 3932160 | tf_op jit(solution)/shard_map/reduce_scatter | solution.py:185
  446.9 0.9 copy-start.5
  496.0 41.0 %copy-start.26 = (bf16[1,2048,768]{2,1,0:T(8,128)(2,1)S(1)}, bf16[1,2048,768]{2,1,0:T(8,128)(2,1)}, u32[]{:S(2)}) copy-start(bf16[1,2048,768]{2,1,0:T(8,128)(2,1)} %param.30) | copy-start | bytes 9437188
  535.3 1.7 copy-start.6
  552.1 82.6 %copy-start.24 = (f32[64,2]{0,1:T(2,128)S(1)}, f32[64,2]{0,1:T(2,128)}, u32[]{:S(2)}) copy-start(f32[64,2]{0,1:T(2,128)} %param.28) | copy-start | bytes 1540
Sparse Core Ops, SparseCore 0:
  13.2 51.5 all-gather.1
  552.2 36.9 reduce-scatter.1
